TPU v7x, 1024 devices: a whole 4x8x16 slice. The times are simulated.
1024 devices in a mesh: rep: 2 (over z_hi), fs: 64 (over z_lo, y), tp: 8 (over x, core).
Axes of the slice: x: 4, y: 8, z: 16 (z_hi: 2, z_lo: 8; z = z_hi * 8 + z_lo), core: 2. Of those that a mesh axis runs over, the one named last changes fastest.
Arguments:
- activations: bfloat16 [2048, 65536], P(None, ('rep', 'fs')), may hold values from -60 to 60
- w_mix_in: bfloat16 [2048, 1024], P('fs', 'tp'), may hold values from -0.125 to 0.125
- w_mix_out: bfloat16 [2048, 1024], P('fs', 'tp'), may hold values from -0.1875 to 0.1875
- w_gate: bfloat16 [2048, 2816], P('fs', 'tp'), may hold values from -0.125 to 0.125
- w_up: bfloat16 [2048, 2816], P('fs', 'tp'), may hold values from -0.125 to 0.125
- w_down: bfloat16 [2048, 2816], P('fs', 'tp'), may hold values from -0.109375 to 0.109375
- pool_scale: float32 [1024], replicated, may hold values from 0.1 to 1.9
- gain_mix: float32 [2048], replicated, may hold values from 0.1 to 1.9
- gain_ffn: float32 [2048], replicated, may hold values from 0.1 to 1.9
- gain_out: float32 [2048], replicated, may hold values from 0.1 to 1.9
Outputs:
- normalized: bfloat16 [2048, 65536], P('tp', ('rep', 'fs'))
All inputs are finite; a program needn't handle non-finite values.
Results may differ from a plain program's by a relative error of at most 0.014.
Values may be sent and summed in bfloat16 or wider, within the bound.
A program may use at most 64 MiB of HBM per device.

v0:
```python
import jax
import jax.numpy as jnp
from jax import lax
from jax.sharding import PartitionSpec as P

POOL_GROUP = 256
SEQ_LEN = 256


EPS = 1e-06
WINDOWS = (2, 4, 8, 16)


def side_by_side(arrays, axis, dim, along):
    ends, at = ([], 0)
    for a in arrays[:-1]:
        at += a.shape[along]
        ends.append(at)
    both = jnp.concatenate(arrays, axis=along)
    return tuple(jnp.split(lax.all_gather(both, axis, axis=dim, tiled=True), ends, axis=along))


def split_up(x, dim, count):
    before, after = (x.shape[:dim], x.shape[dim + 1 :])
    return jnp.moveaxis(x.reshape(*before, count, -1, *after), dim, 0)


def summed_on_arrival(x, axis, dim):
    tiles = split_up(x, dim, lax.axis_size(axis))
    arrived = lax.all_to_all(tiles, axis, split_axis=0, concat_axis=0, tiled=True)
    return arrived.astype(jnp.float32).sum(axis=0)


def copy_for_each(x, axis):
    count = lax.axis_size(axis)
    return lax.all_to_all(jnp.broadcast_to(x[None], (count, *x.shape)), axis, 0, 0, tiled=True)


def taken_together(x, axis):
    return copy_for_each(x, axis).sum(axis=0)


def joined_along(tiles, dim):
    tiles = jnp.moveaxis(tiles, 0, dim)
    lengths = tiles.shape
    return tiles.reshape(*lengths[:dim], lengths[dim] * lengths[dim + 1], *lengths[dim + 2 :])


def collect(x, axis, dim):
    return joined_along(copy_for_each(x, axis), dim)


def rms_factor(stream):
    return lax.rsqrt(jnp.mean(stream * stream, axis=0, keepdims=True) + EPS)


def pool_tokens(inputs, group_of):
    channels = inputs.shape[0]
    values = inputs.astype(jnp.float32).reshape(channels, -1, SEQ_LEN)
    sequences = values.shape[1]
    running = jnp.concatenate(
        [jnp.zeros((channels, sequences, 1), jnp.float32), jnp.cumsum(values, axis=-1)], axis=-1
    )
    places = jnp.arange(SEQ_LEN, dtype=jnp.int32)
    pooled_sum = jnp.zeros_like(values)
    for group_id, window in enumerate(WINDOWS):
        behind = window // 2
        onward = window - behind
        upper_sum = jnp.concatenate(
            [running, jnp.repeat(running[..., -1:], onward, axis=-1)], axis=-1
        )[..., onward : onward + SEQ_LEN]
        lower_sum = jnp.concatenate(
            [jnp.zeros((channels, sequences, behind), jnp.float32), running], axis=-1
        )[..., :SEQ_LEN]
        counts = (jnp.minimum(places + onward, SEQ_LEN) - jnp.maximum(places - behind, 0)).astype(
            jnp.float32
        )
        window_mean = (upper_sum - lower_sum) / counts
        pooled_sum = pooled_sum + jnp.where((group_of == group_id)[:, None, None], window_mean, 0.0)
    return (pooled_sum - values).reshape(channels, -1)


def contract_first(weights, acts):
    return lax.dot_general(
        weights, acts, (((0,), (0,)), ((), ())), preferred_element_type=jnp.float32
    )


def on_device(
    activations, w_mix_in, w_mix_out, w_gate, w_up, w_down, pool_scale, gain_mix, gain_ffn, gain_out
):
    group_size = lax.axis_size("tp")
    group_rank = lax.axis_index("tp")
    features = activations.shape[0]
    feature_share = features // group_size
    feature_start = group_rank * feature_share
    stream = activations.astype(jnp.float32)
    normed = (stream * rms_factor(stream) * gain_mix[:, None]).astype(jnp.bfloat16)
    in_full, out_full = side_by_side((w_mix_in, w_mix_out), "fs", 0, 1)
    inputs = contract_first(in_full, normed).astype(jnp.bfloat16)
    channel_share = w_mix_in.shape[1]
    channel_ids = group_rank * channel_share + jnp.arange(channel_share, dtype=jnp.int32)
    group_of = channel_ids // POOL_GROUP
    scale_own = lax.dynamic_slice_in_dim(pool_scale, group_rank * channel_share, channel_share)
    pooled = (pool_tokens(inputs, group_of) * scale_own[:, None]).astype(jnp.bfloat16)
    stream_own = lax.dynamic_slice_in_dim(stream, feature_start, feature_share, 0)
    mixed_own = summed_on_arrival(
        jnp.dot(out_full, pooled, preferred_element_type=jnp.float32).astype(jnp.bfloat16), "tp", 0
    )
    after_own = lax.optimization_barrier((stream_own + mixed_own).astype(jnp.bfloat16)).astype(
        jnp.float32
    )
    squares = taken_together(jnp.sum(after_own * after_own, axis=0), "tp")
    factor = lax.rsqrt(squares / features + EPS)
    gain_own = lax.dynamic_slice_in_dim(gain_ffn, feature_start, feature_share)
    normed_own = (after_own * factor[None, :] * gain_own[:, None]).astype(jnp.bfloat16)
    normed_two = collect(normed_own, "tp", 0)
    gate_full, up_full, down_full = side_by_side((w_gate, w_up, w_down), "fs", 0, 1)
    gate = contract_first(gate_full, normed_two)
    upward = contract_first(up_full, normed_two)
    hidden = (jax.nn.silu(gate) * upward).astype(jnp.bfloat16)
    ffn_own = summed_on_arrival(
        jnp.dot(down_full, hidden, preferred_element_type=jnp.float32).astype(jnp.bfloat16), "tp", 0
    )
    final_own = after_own + ffn_own
    final_squares = taken_together(jnp.sum(final_own * final_own, axis=0), "tp")
    final_factor = lax.rsqrt(final_squares / features + EPS)
    gain_last = lax.dynamic_slice_in_dim(gain_out, feature_start, feature_share)
    return (final_own * final_factor[None, :] * gain_last[:, None]).astype(jnp.bfloat16)


def solution(mesh):
    placed = (
        P(None, ("rep", "fs")),
        P("fs", "tp"),
        P("fs", "tp"),
        P("fs", "tp"),
        P("fs", "tp"),
        P("fs", "tp"),
        P(),
        P(),
        P(),
        P(),
    )
    return jax.shard_map(
        on_device, mesh=mesh, in_specs=placed, out_specs=P("tp", ("rep", "fs")), check_vma=False
    )
```

profile of v0, /device:TPU:1, one launch (start us, length us, event | category | flops | bytes accessed | tf_op | source)
XLA Modules:
  0.0 945.2 jit_solution(13969995607842278405)
XLA Ops:
  6.5 0.0 copy-start
  6.5 0.0 copy-start.2
  6.5 0.0 all-gather.3.cloned.1.call-start
  6.5 1.5 pad_maximum_fusion.11
  8.0 0.0 all-gather.3.cloned.1.call-update
  8.0 0.0 all-gather.5.cloned.1.call-start
  8.1 1.5 concatenate.46
  9.6 0.0 all-gather.5.cloned.1.call-update
  9.6 0.8 dynamic_slice.13
  10.5 2.1 multiply_reduce_fusion
  12.6 391.5 %all-gather.3.cloned.1.call-done = bf16[2048,256]{1,0:T(8,128)(2,1)} async-done(((bf16[32,256]{1,0:T(8,128)(2,1)}), bf16[2048,256]{1,0:T(8,128)(2,1)}) %all-gather.3.cloned.1.call-update) | async-done | bytes 1048592 | tf_op jit(solution)/shard_map/all_gather | solution.py:20
  404.1 0.0 copy-done
  404.1 0.0 copy-done.2
  404.1 1.9 fusion.16
  406.0 0.2 reshape.142
  406.2 0.1 copy.23
  406.3 0.2 copy.18
  406.6 0.1 fusion.64
  406.8 0.0 copy-start.1
  406.8 0.1 broadcast_add_fusion
  406.9 0.4 fusion.34
  407.4 0.6 copy-done.1
  408.0 2.1 convolution_convert_fusion
  410.0 52.9 %all-to-all-start = ((bf16[8,256,512]{2,1,0:T(8,128)(2,1)}), bf16[8,256,512]{2,1,0:T(8,128)(2,1)}, u32[]{:S(2)}, u32[]{:S(2)}) async-start(bf16[8,256,512]{2,1,0:T(8,128)(2,1)} %bitcast.16), calls=%async_computation | async-start | bytes 4194304 | tf_op jit(solution)/shard_map/all_to_all | solution.py:30
  462.9 2.6 convert_element_type.70
  465.6 23.7 %all-to-all-done = bf16[8,256,512]{2,1,0:T(8,128)(2,1)} async-done(((bf16[8,256,512]{2,1,0:T(8,128)(2,1)}), bf16[8,256,512]{2,1,0:T(8,128)(2,1)}, u32[]{:S(2)}, u32[]{:S(2)}) %all-to-all-start) | async-done | bytes 2097184 | tf_op jit(solution)/shard_map/all_to_all | solution.py:30
  489.3 1.9 convert_reduce_fusion.1
  491.2 1.1 add_convert_fusion
  492.3 0.1 fusion.24
  492.4 0.6 broadcast_in_dim.83
  493.0 4.2 all-to-all-start.1
  497.2 0.8 dynamic_slice.14
  498.0 4.3 all-to-all-done.1
  502.3 0.1 fusion.26
  502.4 0.2 broadcast_in_dim.84
  502.6 29.3 %all_to_all.27 = bf16[8,256,512]{2,1,0:T(8,128)(2,1)S(1)} all-to-all(bf16[8,256,512]{2,1,0:T(8,128)(2,1)S(1)} %broadcast_in_dim.84), channel_id=1, replica_groups=mesh['rep'=2,'fs'=64,'tp'=8] {'tp'}, dimensions={0} | all-to-all | bytes 4194304 | tf_op jit(solution)/shard_map/all_to_all | solution.py:36
  531.9 309.1 %all-gather.5.cloned.1.call-done = bf16[2048,1056]{1,0:T(8,128)(2,1)} async-done(((bf16[32,1056]{1,0:T(8,128)(2,1)}), bf16[2048,1056]{1,0:T(8,128)(2,1)}) %all-gather.5.cloned.1.call-update) | async-done | bytes 4325392 | tf_op jit(solution)/shard_map/all_gather | solution.py:20
  841.1 2.3 fusion.6
  843.4 6.5 convolution_convert_fusion.1
  849.9 77.7 %all_to_all.28 = bf16[8,256,512]{2,1,0:T(8,128)(2,1)S(1)} all-to-all(bf16[8,256,512]{2,1,0:T(8,128)(2,1)} %bitcast.19), channel_id=1, replica_groups=mesh['rep'=2,'fs'=64,'tp'=8] {'tp'}, dimensions={0} | all-to-all | bytes 4194304 | tf_op jit(solution)/shard_map/all_to_all | solution.py:30
  927.6 0.3 convert_reduce_fusion
  927.9 0.1 multiply_reduce_fusion.1
  928.0 0.6 broadcast_in_dim.85
  928.6 4.3 all-to-all-start.4
  932.9 0.8 dynamic_slice.15
  933.6 3.9 all-to-all-done.4
  937.6 0.8 multiply_convert_fusion.6
  (24 shorter events, 0.2 us)
Async XLA Ops:
  6.5 397.6 %copy-start = (bf16[2048,512]{1,0:T(8,128)(2,1)S(1)}, bf16[2048,512]{1,0:T(8,128)(2,1)}, u32[]{:S(2)}) copy-start(bf16[2048,512]{1,0:T(8,128)(2,1)} %param.10) | copy-start | bytes 6291460
  6.5 397.6 %copy-start.2 = (f32[2048]{0:T(1024)S(1)}, f32[2048]{0:T(1024)}, u32[]{:S(2)}) copy-start(f32[2048]{0:T(1024)} %param.17) | copy-start | bytes 24580
  6.5 397.6 %all-gather.3.cloned.1.call-start = ((), (), s32[]{:S(2)}) async-start(), calls=%async_computation.5 | async-start | bytes 1064960 | tf_op jit(solution)/shard_map/all_gather | solution.py:20
  8.0 833.0 %all-gather.5.cloned.1.call-start = ((), (), s32[]{:S(2)}) async-start(), calls=%async_computation.6 | async-start | bytes 4792320 | tf_op jit(solution)/shard_map/all_gather | solution.py:20
  406.8 1.2 copy-start.1
  410.0 79.2 %all-to-all-start = ((bf16[8,256,512]{2,1,0:T(8,128)(2,1)}), bf16[8,256,512]{2,1,0:T(8,128)(2,1)}, u32[]{:S(2)}, u32[]{:S(2)}) async-start(bf16[8,256,512]{2,1,0:T(8,128)(2,1)} %bitcast.16), calls=%async_computation | async-start | bytes 4194304 | tf_op jit(solution)/shard_map/all_to_all | solution.py:30
  493.0 9.2 all-to-all-start.1
  928.6 9.0 all-to-all-start.4
Sparse Core Ops, SparseCore 0:
  10.0 394.0 all-gather.2
  406.8 434.2 all-gather.4
where the time goes:
time: 946 us; the launch traced here: 945 us
  waiting for transfers between devices  733 us (77%)
  blocking collectives  107 us (11%)
  starting transfers between devices  61.4 us (6%)
  between operations  13.6 us (1%)
  matrix products  12.8 us (1%)
  other arithmetic  11.5 us (1%)
    all_gather x2, waiting for transfers between devices, side_by_side(): lax.all_gather(both, axis, axis=dim, tiled=True)  701 us
    all_to_all x1, blocking collectives, summed_on_arrival(): lax.all_to_all(tiles, axis, split_axis=0, concat_axis=0, tiled=True)  77.7 us
    all_to_all x1, starting transfers between devices, summed_on_arrival(): lax.all_to_all(tiles, axis, split_axis=0, concat_axis=0, tiled=True)  52.9 us
    all_to_all x1, blocking collectives, copy_for_each(): lax.all_to_all(jnp.broadcast_to(x[None], (count, *x.shape)), axis, 0, 0,...  29.3 us
    all_to_all x1, waiting for transfers between devices, summed_on_arrival(): lax.all_to_all(tiles, axis, split_axis=0, concat_axis=0, tiled=True)  23.7 us
  transfers between devices with their start and end apart: 5, of which 5 were waited for; matrix products, arithmetic and copies ran while one was open for 2% of the time, Pallas kernels for 0%

commit v1 on v0

v1 whole, which is shorter than its diff:
```python
import jax
import jax.numpy as jnp
from jax import lax
from jax.experimental import pallas as pl
from jax.experimental.pallas import tpu as pltpu
from jax.sharding import PartitionSpec as P

F32 = jnp.float32
BF16 = jnp.bfloat16
SEQ = 256
EPS = 1e-06
TOK = 512
D = 2048
HID = 384
MESH = pl.DeviceIdType.MESH
MIX_IN, MIX_OUT, GATE, UP, DOWN = range(5)
HALVES = (1, 2, 1, 1, 2)


def wide(tile, times):
    return jnp.concatenate([tile] * times, axis=1)


def spread_row(row):
    return jnp.transpose(jnp.broadcast_to(row, (128, 128)))


def dot(a, b):
    return jnp.dot(a, b, preferred_element_type=F32)


def dot_first(a, b):
    return lax.dot_general(a, b, (((0,), (0,)), ((), ())), preferred_element_type=F32)


def kernel(
    x_hbm, wi_hbm, wo_hbm, wf_hbm, scale_ref, g1_ref, g2_ref, g3_ref,
    out_ref,
    xb, hb, x1b, mb, ob, opb, gb, ub, db, pc, pp, gcol, hid,
    to_pair, from_pair, own, far2, rgt, lft, keep_r, keep_l, in_l, in_r, in_far, ssq,
    loc_sem, p1_send, p1_recv, p2_send, p2_recv, xo_send, xo_recv, d2_send, d2_recv,
    p_send, p_recv, rs_send, rs_recv, q_send, q_recv,
):
    rep, fs, tp = lax.axis_index("rep"), lax.axis_index("fs"), lax.axis_index("tp")
    zl, y = fs // 8, fs % 8
    z = rep * 8 + zl
    x, c = tp // 2, tp % 2
    a_own = y + c * (zl - y)
    b_own = zl + c * (y - zl)

    def device(zz, yy, xx, cc):
        zz = (zz + 32) % 16
        yy = (yy + 16) % 8
        return (zz // 8, (zz % 8) * 8 + yy, ((xx + 8) % 4) * 2 + cc)

    def ring_a(d):
        return device(z + c * d, y + (1 - c) * d, x, c)

    def ring_b(d):
        return device(z + (1 - c) * d, y + c * d, x, c)

    def fidx(b, a):
        return (b * 8 + a) + c * ((a * 8 + b) - (b * 8 + a))

    started = []

    def remote(src, dst, send, recv, dev):
        return pltpu.make_async_remote_copy(
            src_ref=src, dst_ref=dst, send_sem=send, recv_sem=recv, device_id=dev, device_id_type=MESH
        )

    def go(copy):
        copy.start()
        started.append(copy)

    bufs = (mb, ob, gb, ub, db)

    locals_ = [
        pltpu.make_async_copy(wi_hbm, mb.at[b_own, a_own], loc_sem.at[0]),
        pltpu.make_async_copy(
            wo_hbm, ob.at[b_own, a_own, :, pl.ds(pl.multiple_of(x * 128, 128), 128)], loc_sem.at[1]
        ),
        pltpu.make_async_copy(wf_hbm.at[0], gb.at[b_own, a_own], loc_sem.at[2]),
        pltpu.make_async_copy(wf_hbm.at[1], ub.at[b_own, a_own], loc_sem.at[3]),
        pltpu.make_async_copy(wf_hbm.at[2], db.at[b_own, a_own], loc_sem.at[4]),
    ]
    x_copy = pltpu.make_async_copy(x_hbm, xb, loc_sem.at[5])
    for cp in locals_:
        cp.start()
    x_copy.start()
    barrier = pltpu.get_barrier_semaphore()
    peers = [ring_a(d) for d in (1, -1, 2, -2, 3, -3, 4, -4)] + [ring_b(1), ring_b(-1)]
    peers += [device(z, y, x + dx, cc) for dx in (1, 2, 3) for cc in (c, 1 - c)]
    peers += [device(z, y, x, 1 - c)]
    for dev in peers:
        pl.semaphore_signal(barrier, inc=1, device_id=dev, device_id_type=MESH)
    for cp in locals_:
        cp.wait()
    pl.semaphore_wait(barrier, len(peers))

    offsets = (1, -1, 2, -2, 3, -3, 4)

    def p1(t, i):
        blk = bufs[t].at[b_own, a_own]
        return remote(blk, blk, p1_send.at[t, i], p1_recv.at[t, i], ring_a(offsets[i]))

    def p1_start(t):
        for i in range(7):
            go(p1(t, i))

    def p1_wait(t):
        for i in range(7):
            src = (a_own - offsets[i] + 8) % 8
            blk = bufs[t].at[b_own, src]
            remote(blk, blk, p1_send.at[t, i], p1_recv.at[t, i], ring_a(0 - offsets[i])).wait_recv()

    p1_start(MIX_IN)
    wo_dst = ob.at[b_own, a_own, :, pl.ds(pl.multiple_of(x * 128, 128), 128)]
    for dx in (1, 3, 2):
        go(remote(wo_dst, wo_dst, xo_send.at[dx - 1], xo_recv.at[dx - 1], device(z, y, x + dx, c)))
    p1_start(GATE)

    def spread_gain(g_ref):
        for r in range(16):
            gcol[4 * r : 4 * r + 4] = spread_row(g_ref[r : r + 1, :]).reshape(4, 32, 128)

    def add_squares(acc, v):
        return acc + (v * v).reshape(4, 8, TOK).sum(axis=0)

    def factor(acc):
        return lax.rsqrt(jnp.sum(acc, axis=0, keepdims=True) / D + EPS)

    x_copy.wait()
    spread_gain(g1_ref)
    acc1 = lax.fori_loop(
        0, 64, lambda i, acc: add_squares(acc, xb[i].astype(F32)), jnp.zeros((8, TOK), F32)
    )
    r1 = factor(acc1)

    for dx in (1, 3, 2):
        xs = (x - dx + 4) % 4
        got = ob.at[b_own, a_own, :, pl.ds(pl.multiple_of(xs * 128, 128), 128)]
        remote(got, got, xo_send.at[dx - 1], xo_recv.at[dx - 1], device(z, y, x, c)).wait_recv()
    p1_start(MIX_OUT)
    p1_start(UP)
    p1_start(DOWN)

    def row_part(t, row, d, way, half):
        if d == 3:
            return bufs[t].at[row, pl.ds(0, 4)] if way == 1 else bufs[t].at[row, pl.ds(4, 4)]
        if HALVES[t] == 2:
            return bufs[t].at[row, pl.ds(4 * half, 4)]
        return bufs[t].at[row]

    def p2(t, d, way, half, arriving):
        w = (1 - way) // 2
        row = (b_own - way * (d + arriving) + 16) % 8
        part = row_part(t, row, d, way, half)
        at = d * 2 + half
        return remote(part, part, p2_send.at[t, w, at], p2_recv.at[t, w, at], ring_b(way))

    def parts_of(t, d):
        return range(1 if d == 3 else HALVES[t])

    def forward(t, d, half=0):
        for way in (1, -1):
            if d in (1, 2):
                p2(t, d - 1, way, half, 1).wait_recv()
            elif d == 3:
                own_half = 0 if way == 1 else 1
                if HALVES[t] == 2:
                    p2(t, 2, way, own_half, 1).wait_recv()
                else:
                    p2(t, 2, way, 0, 1).wait_recv()
            go(p2(t, d, way, half, 0))
        if d == 3 and HALVES[t] == 2:
            for way in (1, -1):
                other_half = 1 if way == 1 else 0
                p2(t, 2, way, other_half, 1).wait_recv()

    def last(t):
        for way in (1, -1):
            p2(t, 3, way, 0, 1).wait_recv()

    pair = device(z, y, x, 1 - c)

    def to_pair_row(k):
        row = (b_own - k + 16) % 8
        return remote(ob.at[row], opb.at[:, row], d2_send.at[k], d2_recv.at[k], pair)

    p1_wait(MIX_IN)
    forward(MIX_IN, 0)
    p1_wait(MIX_OUT)
    forward(MIX_OUT, 0, 0)

    def scale_h(src, fac):
        def body(i, carry):
            v = src[i].astype(F32) * fac * wide(gcol[i], 4)
            b, a = i // 8, i % 8
            hb[fidx(b, a)] = v.astype(BF16)
            return carry

        lax.fori_loop(0, 64, body, 0)

    scale_h(xb, r1)
    forward(MIX_IN, 1)
    forward(MIX_OUT, 0, 1)
    go(to_pair_row(0))
    forward(MIX_IN, 2)
    p1_wait(GATE)
    forward(GATE, 0)
    forward(MIX_IN, 3)
    forward(MIX_OUT, 1, 0)
    forward(MIX_OUT, 1, 1)
    go(to_pair_row(1))
    go(to_pair_row(7))
    spread_gain(g2_ref)
    last(MIX_IN)

    u = dot_first(mb[...].reshape(D, 128), hb[...].reshape(D, TOK)).astype(BF16)
    behind = lax.shift_left(jnp.int32(1), x.astype(jnp.int32))
    src_place = lax.broadcasted_iota(jnp.int32, (SEQ, SEQ), 0)
    dst_place = lax.broadcasted_iota(jnp.int32, (SEQ, SEQ), 1)
    inside = (src_place >= dst_place - behind) & (src_place < dst_place + behind)
    band = jnp.where(inside, 1.0, 0.0).astype(BF16)
    place = lax.broadcasted_iota(jnp.int32, (1, SEQ), 1)
    counts = (jnp.minimum(place + behind, SEQ) - jnp.maximum(place - behind, 0)).astype(F32)
    scale_col = wide(spread_row(scale_ref[pl.ds(tp, 1), :]), 2)
    for s in range(2):
        us = u[:, s * SEQ : (s + 1) * SEQ]
        mean = dot(us, band) / counts
        pc[x, :, s * SEQ : (s + 1) * SEQ] = ((mean - us.astype(F32)) * scale_col).astype(BF16)

    right, left = device(z, y, x + 1, c), device(z, y, x - 1, c)
    xr, xl, xo = (x + 1) % 4, (x + 3) % 4, (x + 2) % 4
    p1_wait(UP)
    forward(UP, 0)
    go(remote(pc.at[x], pc.at[x], p_send.at[0], p_recv.at[0], right))
    go(remote(pc.at[x], pc.at[x], p_send.at[1], p_recv.at[1], left))
    go(remote(pc.at[x], pp.at[x], p_send.at[2], p_recv.at[2], pair))
    forward(MIX_OUT, 2, 0)
    forward(MIX_OUT, 2, 1)
    go(to_pair_row(2))
    go(to_pair_row(6))
    forward(GATE, 1)
    remote(pc.at[xl], pc.at[xl], p_send.at[0], p_recv.at[0], right).wait_recv()
    lo, hi = pl.ds(0, 64), pl.ds(64, 64)
    go(remote(pc.at[xl, lo], pc.at[xl, lo], p_send.at[3], p_recv.at[3], right))
    go(remote(pc.at[xl], pp.at[xl], p_send.at[4], p_recv.at[4], pair))
    remote(pc.at[xr], pc.at[xr], p_send.at[1], p_recv.at[1], left).wait_recv()
    go(remote(pc.at[xr, hi], pc.at[xr, hi], p_send.at[5], p_recv.at[5], left))
    go(remote(pc.at[xr], pp.at[xr], p_send.at[6], p_recv.at[6], pair))
    forward(MIX_OUT, 3)
    go(to_pair_row(3))
    go(to_pair_row(5))
    forward(UP, 1)
    p1_wait(DOWN)
    remote(pc.at[xo, lo], pc.at[xo, lo], p_send.at[3], p_recv.at[3], right).wait_recv()
    remote(pc.at[xo, hi], pc.at[xo, hi], p_send.at[5], p_recv.at[5], left).wait_recv()
    go(remote(pc.at[xo], pp.at[xo], p_send.at[7], p_recv.at[7], pair))
    forward(GATE, 2)
    last(MIX_OUT)
    go(to_pair_row(4))
    forward(UP, 2)
    forward(DOWN, 0, 0)
    forward(DOWN, 0, 1)
    for n, at in ((2, x), (4, xl), (6, xr), (7, xo)):
        remote(pc.at[at], pp.at[at], p_send.at[n], p_recv.at[n], pair).wait_recv()
    for k in range(8):
        row = (a_own - k + 16) % 8
        remote(ob.at[row], opb.at[:, row], d2_send.at[k], d2_recv.at[k], pair).wait_recv()

    def mix_row(b, acc):
        m = dot(ob[b].reshape(256, 512), pc[...].reshape(512, TOK))
        m = m + dot(opb[b].reshape(256, 512), pp[...].reshape(512, TOK))
        for a in range(8):
            f = fidx(b, a)
            v = (xb[f].astype(F32) + m[a * 32 : (a + 1) * 32]).astype(BF16)
            x1b[f] = v
            acc = add_squares(acc, v.astype(F32))
        return acc

    acc2 = lax.fori_loop(0, 8, mix_row, jnp.zeros((8, TOK), F32))
    forward(GATE, 3)
    forward(UP, 3)
    forward(DOWN, 1, 0)
    forward(DOWN, 1, 1)
    scale_h(x1b, factor(acc2))
    forward(DOWN, 2, 0)
    forward(DOWN, 2, 1)
    last(GATE)
    last(UP)
    forward(DOWN, 3)

    def hidden_half(n, carry):
        at = pl.ds(pl.multiple_of(n * 256, 256), 256)
        rhs = hb[:, :, at].reshape(D, 256)
        g = dot_first(gb[...].reshape(D, HID), rhs)
        v = dot_first(ub[...].reshape(D, HID), rhs)
        hid[:, at] = (g / (1.0 + jnp.exp(-g)) * v).astype(BF16)
        return carry

    lax.fori_loop(0, 2, hidden_half, 0)
    last(DOWN)

    def term(xd, cd):
        t = xd * 2 + cd
        rows = [db[t + c * (i - t), i + c * (t - i)] for i in range(8)]
        return dot(jnp.concatenate(rows, axis=0), hid[...])

    def pair_copy(j):
        return remote(to_pair.at[j], from_pair.at[j], rs_send.at[j], rs_recv.at[j], pair)

    dests = (xo, xr, xl, x)
    to_pair[0] = term(xo, 1 - c).astype(BF16)
    to_pair[1] = term(xr, 1 - c).astype(BF16)
    go(pair_copy(0))
    to_pair[2] = term(xl, 1 - c).astype(BF16)
    go(pair_copy(1))
    to_pair[3] = term(x, 1 - c).astype(BF16)
    go(pair_copy(2))
    own[...] = term(xo, c)
    go(pair_copy(3))
    pair_copy(0).wait_recv()
    far2[...] = (own[...] + from_pair[0].astype(F32)).astype(BF16).reshape(2, 128, TOK)
    own[...] = term(xr, c)
    far_r = remote(far2.at[0], in_far.at[0], rs_send.at[4], rs_recv.at[4], right)
    far_l = remote(far2.at[1], in_far.at[1], rs_send.at[5], rs_recv.at[5], left)
    go(far_r)
    go(far_l)
    pair_copy(1).wait_recv()
    keep_r[...] = own[0:128] + from_pair[1, 0:128].astype(F32)
    rgt[1] = (own[128:256] + from_pair[1, 128:256].astype(F32)).astype(BF16)
    own[...] = term(xl, c)
    r_plain = remote(rgt.at[1], in_l.at[1], rs_send.at[6], rs_recv.at[6], right)
    go(r_plain)
    pair_copy(2).wait_recv()
    keep_l[...] = own[128:256] + from_pair[2, 128:256].astype(F32)
    lft[0] = (own[0:128] + from_pair[2, 0:128].astype(F32)).astype(BF16)
    own[...] = term(x, c)
    l_plain = remote(lft.at[0], in_r.at[0], rs_send.at[7], rs_recv.at[7], left)
    go(l_plain)
    pair_copy(3).wait_recv()
    for a in range(8):
        at = slice(a * 32, (a + 1) * 32)
        own[at] = own[at] + from_pair[3, at].astype(F32) + x1b[tp * 8 + a].astype(F32)
    far_r.wait_recv()
    rgt[0] = (keep_r[...] + in_far[0].astype(F32)).astype(BF16)
    r_sum = remote(rgt.at[0], in_l.at[0], rs_send.at[8], rs_recv.at[8], right)
    go(r_sum)
    far_l.wait_recv()
    lft[1] = (keep_l[...] + in_far[1].astype(F32)).astype(BF16)
    l_sum = remote(lft.at[1], in_r.at[1], rs_send.at[9], rs_recv.at[9], left)
    go(l_sum)
    r_plain.wait_recv()
    l_plain.wait_recv()
    own[128:256] = own[128:256] + in_l[1].astype(F32)
    own[0:128] = own[0:128] + in_r[0].astype(F32)
    r_sum.wait_recv()
    l_sum.wait_recv()
    own[0:128] = own[0:128] + in_l[0].astype(F32)
    own[128:256] = own[128:256] + in_r[1].astype(F32)

    total = jnp.sum(own[...] * own[...], axis=0, keepdims=True)
    ssq[tp] = total

    def q_copy(o, at):
        t = (tp + o) % 8
        return remote(ssq.at[at], ssq.at[at], q_send.at[o - 1], q_recv.at[o - 1], device(z, y, t // 2, t % 2))

    gain3 = jnp.concatenate(
        [wide(spread_row(g3_ref[pl.ds(tp * 2 + i, 1), :]), 4) for i in range(2)], axis=0
    )
    for o in range(1, 8):
        go(q_copy(o, tp))
    for o in range(1, 8):
        q_copy(o, (tp - o + 8) % 8).wait_recv()
    squares = ssq[0]
    for k in range(1, 8):
        squares = squares + ssq[k]
    fac = lax.rsqrt(squares / D + EPS)
    out_ref[...] = (own[...] * fac * gain3).astype(BF16)
    for copy in started:
        copy.wait_send()


def on_device(
    activations, w_mix_in, w_mix_out, w_gate, w_up, w_down, pool_scale, gain_mix, gain_ffn, gain_out
):
    pad = ((0, 0), (0, HID - w_gate.shape[1]))
    wf = jnp.stack([jnp.pad(w, pad) for w in (w_gate, w_up, w_down)])
    vmem = pl.BlockSpec(memory_space=pltpu.VMEM)
    hbm = pl.BlockSpec(memory_space=pl.ANY)
    dma = pltpu.SemaphoreType.DMA
    rows = lambda width: pltpu.VMEM((8, 8, 32, width), BF16)
    return pl.pallas_call(
        kernel,
        out_shape=jax.ShapeDtypeStruct((256, TOK), BF16),
        in_specs=[hbm] * 4 + [vmem] * 4,
        out_specs=vmem,
        scratch_shapes=[
            pltpu.VMEM((64, 32, TOK), BF16),
            pltpu.VMEM((64, 32, TOK), BF16),
            pltpu.VMEM((64, 32, TOK), BF16),
            rows(128), rows(512), rows(512), rows(HID), rows(HID), rows(HID),
            pltpu.VMEM((4, 128, TOK), BF16),
            pltpu.VMEM((4, 128, TOK), BF16),
            pltpu.VMEM((64, 32, 128), F32),
            pltpu.VMEM((HID, TOK), BF16),
            pltpu.VMEM((4, 256, TOK), BF16),
            pltpu.VMEM((4, 256, TOK), BF16),
            pltpu.VMEM((256, TOK), F32),
            pltpu.VMEM((2, 128, TOK), BF16),
            pltpu.VMEM((2, 128, TOK), BF16),
            pltpu.VMEM((2, 128, TOK), BF16),
            pltpu.VMEM((128, TOK), F32),
            pltpu.VMEM((128, TOK), F32),
            pltpu.VMEM((2, 128, TOK), BF16),
            pltpu.VMEM((2, 128, TOK), BF16),
            pltpu.VMEM((2, 128, TOK), BF16),
            pltpu.VMEM((8, 1, TOK), F32),
            dma((6,)),
            dma((5, 7)), dma((5, 7)),
            dma((5, 2, 8)), dma((5, 2, 8)),
            dma((3,)), dma((3,)),
            dma((8,)), dma((8,)),
            dma((8,)), dma((8,)),
            dma((10,)), dma((10,)),
            dma((7,)), dma((7,)),
        ],
        compiler_params=pltpu.CompilerParams(
            collective_id=0, has_side_effects=True, vmem_limit_bytes=60 * 1024 * 1024
        ),
        name="layer",
    )(
        activations.reshape(64, 32, TOK), w_mix_in, w_mix_out, wf,
        pool_scale.reshape(8, 128), gain_mix.reshape(16, 128),
        gain_ffn.reshape(16, 128), gain_out.reshape(16, 128),
    )


def solution(mesh):
    shards = P("fs", "tp")
    placed = (P(None, ("rep", "fs")),) + (shards,) * 5 + (P(),) * 4
    return jax.shard_map(
        on_device, mesh=mesh, in_specs=placed, out_specs=P("tp", ("rep", "fs")), check_vma=False
    )
```

time: 946 us -> 102 us (0.11)
  waiting for transfers between devices: 733 us -> 0 us
  blocking collectives: 107 us -> 0 us
  Pallas kernels: 0 us -> 98.1 us
  starting transfers between devices: 61.4 us -> 0 us
  between operations: 13.6 us -> 0.01 us
  matrix products: 12.8 us -> 0 us
  other arithmetic: 11.5 us -> 0.64 us
    all_gather x2 -> x0, waiting for transfers between devices: 701 us -> none  [side_by_side(): lax.all_gather(both, axis, axis=dim, tiled=True)]
    all_to_all x2 -> x0, blocking collectives: 107 us -> none  [the longest x1 77.7 us: summed_on_arrival(): lax.all_to_all(tiles, axis, split_axis=0, concat_axis=0, tiled=True)]
    pallas_call x0 -> x1, Pallas kernels: none -> 98.1 us  [on_device(): pl.pallas_call(kernel, out_shape=jax.ShapeDtypeStruct((256, TOK), BF16),...]
    all_to_all x3 -> x0, starting transfers between devices: 61.4 us -> none  [the longest x1 52.9 us: summed_on_arrival(): lax.all_to_all(tiles, axis, split_axis=0, concat_axis=0, tiled=True)]
    all_to_all x3 -> x0, waiting for transfers between devices: 32 us -> none  [the longest x1 23.7 us: summed_on_arrival(): lax.all_to_all(tiles, axis, split_axis=0, concat_axis=0, tiled=True)]
    dot_general x4 -> x0, matrix products: 12.8 us -> none  [the longest x1 6.5 us: on_device(): jnp.dot(down_full, hidden, preferred_element_type=jnp.float32)]
  transfers between devices with their start and end apart: 5 -> 0, of which waited for: 5 -> 0; matrix products, arithmetic and copies ran while one was open for 2% -> 0% of each run, Pallas kernels for 0% -> 0%
where the time goes in v1:
time: 102 us
  Pallas kernels  98.1 us (96%)
  local copies, waits for them, and re-layouts  3.18 us (3%)
    pallas_call x1, Pallas kernels, on_device(): pl.pallas_call(kernel, out_shape=jax.ShapeDtypeStruct((256, TOK), BF16),...  98.1 us

profile of v1, /device:TPU:1, one launch (start us, length us, event | category | flops | bytes accessed | tf_op | source)
XLA Modules:
  0.0 102.0 jit_solution(13163881698481086316)
XLA Ops:
  0.0 0.7 pad_bitcast_fusion.2
  0.7 0.8 pad_bitcast_fusion
  1.5 0.6 pad_maximum_fusion.wf_hbm
  2.2 98.1 %layer.1 = bf16[256,512]{1,0:T(8,128)(2,1)} custom-call(bf16[64,32,512]{2,1,0:T(8,128)(2,1)} %bitcast.11, bf16[32,128]{1,0:T(8,128)(2,1)} %wi_hbm.1, bf16[32,128]{1,0:T(8,128)(2,1)} %wo_hbm.1, bf16[3,32,384]{2,1,0:T(8,128)(2,1)} %pad_maximum_fusion.wf_hbm, f32[8,128]{1,0:T(8,128)} %bitcast.15, f32[16,128]{1,0:T(8,128)} %bitcast.12, f32[16,128]{1,0:T(8,128)} %bitcast.13, ...), custom_call_target="tpu_custom_call" | custom-call | tf_op jit(solution)/shard_map/layer/pallas_call | solution.py:396
  100.3 1.7 %copy.12 = bf16[256,512]{1,0:T(8,128)(2,1)} copy(bf16[256,512]{1,0:T(8,128)(2,1)} %layer.1) | data formatting | bytes 524288

commit v2 on v1

--- a/solution.py
+++ b/solution.py
@@ -14,7 +14,8 @@
 HID = 384
 MESH = pl.DeviceIdType.MESH
 MIX_IN, MIX_OUT, GATE, UP, DOWN = range(5)
-HALVES = (1, 2, 1, 1, 2)
+HALVES = (1, 1, 2, 2, 2)
+CHUNKS = ((0, 1, 7), (2, 6), (3, 4, 5))
 
 
 def wide(tile, times):
@@ -34,11 +35,11 @@
 
 
 def kernel(
-    x_hbm, wi_hbm, wo_hbm, wf_hbm, scale_ref, g1_ref, g2_ref, g3_ref,
+    x_hbm, wi_hbm, wo_hbm, wg_ref, wu_ref, wd_ref, scale_ref, g1_ref, g2_ref, g3_ref,
     out_ref,
-    xb, hb, x1b, mb, ob, opb, gb, ub, db, pc, pp, gcol, hid,
+    xb, hb, x1b, mb, ob, opb, gb, ub, db, pc, pp, gcol, hid, g_acc, u_acc,
     to_pair, from_pair, own, far2, rgt, lft, keep_r, keep_l, in_l, in_r, in_far, ssq,
-    loc_sem, p1_send, p1_recv, p2_send, p2_recv, xo_send, xo_recv, d2_send, d2_recv,
+    loc_sem, p1_send, p1_recv, p1r_recv, p2_send, p2_recv, xo_send, xo_recv, d2_send, d2_recv,
     p_send, p_recv, rs_send, rs_recv, q_send, q_recv,
 ):
     rep, fs, tp = lax.axis_index("rep"), lax.axis_index("fs"), lax.axis_index("tp")
@@ -73,18 +74,22 @@
         copy.start()
         started.append(copy)
 
-    bufs = (mb, ob, gb, ub, db)
+    def drain(keep):
+        for _ in range(len(started) - keep):
+            started.pop(0).wait_send()
+
+    def lane(xx):
+        return pl.ds(pl.multiple_of(xx * 128, 128), 128)
+
+    bufs = (mb, ob.at[:, :, :, lane(x)], gb, ub, db)
 
     locals_ = [
         pltpu.make_async_copy(wi_hbm, mb.at[b_own, a_own], loc_sem.at[0]),
         pltpu.make_async_copy(
-            wo_hbm, ob.at[b_own, a_own, :, pl.ds(pl.multiple_of(x * 128, 128), 128)], loc_sem.at[1]
+            wo_hbm, ob.at[b_own, a_own, :, lane(x)], loc_sem.at[1]
         ),
-        pltpu.make_async_copy(wf_hbm.at[0], gb.at[b_own, a_own], loc_sem.at[2]),
-        pltpu.make_async_copy(wf_hbm.at[1], ub.at[b_own, a_own], loc_sem.at[3]),
-        pltpu.make_async_copy(wf_hbm.at[2], db.at[b_own, a_own], loc_sem.at[4]),
     ]
-    x_copy = pltpu.make_async_copy(x_hbm, xb, loc_sem.at[5])
+    x_copy = pltpu.make_async_copy(x_hbm, xb, loc_sem.at[2])
     for cp in locals_:
         cp.start()
     x_copy.start()
@@ -94,31 +99,48 @@
     peers += [device(z, y, x, 1 - c)]
     for dev in peers:
         pl.semaphore_signal(barrier, inc=1, device_id=dev, device_id_type=MESH)
+    for buf, ref in ((gb, wg_ref), (ub, wu_ref), (db, wd_ref)):
+        width = ref.shape[1]
+        buf[b_own, a_own, :, 0:width] = ref[...]
+        buf[b_own, a_own, :, width:HID] = jnp.zeros((32, HID - width), BF16)
     for cp in locals_:
         cp.wait()
     pl.semaphore_wait(barrier, len(peers))
 
     offsets = (1, -1, 2, -2, 3, -3, 4)
 
-    def p1(t, i):
+    def p1_start(t):
         blk = bufs[t].at[b_own, a_own]
-        return remote(blk, blk, p1_send.at[t, i], p1_recv.at[t, i], ring_a(offsets[i]))
-
-    def p1_start(t):
-        for i in range(7):
-            go(p1(t, i))
+        for d in offsets:
+            remote(blk, blk, p1_send.at[t], p1_recv.at[t], ring_a(d)).start()
 
     def p1_wait(t):
-        for i in range(7):
-            src = (a_own - offsets[i] + 8) % 8
-            blk = bufs[t].at[b_own, src]
-            remote(blk, blk, p1_send.at[t, i], p1_recv.at[t, i], ring_a(0 - offsets[i])).wait_recv()
+        blks = bufs[t].at[b_own, pl.ds(0, 7)]
+        remote(blks, blks, p1_send.at[t], p1_recv.at[t], ring_a(1)).wait_recv()
+
+    def ring_1(t, d, way, arriving):
+        w = (1 - way) // 2
+        at = (a_own - way * (d + arriving) + 16) % 8
+        blk = bufs[t].at[b_own, at]
+        if d == 3:
+            blk = bufs[t].at[b_own, at, pl.ds(0 if way == 1 else 16, 16)]
+        return remote(blk, blk, p1_send.at[t], p1r_recv.at[t - UP, w * 4 + d], ring_a(way))
+
+    def p1_ring(t, d):
+        for way in (1, -1):
+            if d:
+                ring_1(t, d - 1, way, 1).wait_recv()
+            ring_1(t, d, way, 0).start()
+
+    def p1_ring_last(t):
+        for way in (1, -1):
+            ring_1(t, 3, way, 1).wait_recv()
 
     p1_start(MIX_IN)
-    wo_dst = ob.at[b_own, a_own, :, pl.ds(pl.multiple_of(x * 128, 128), 128)]
-    for dx in (1, 3, 2):
-        go(remote(wo_dst, wo_dst, xo_send.at[dx - 1], xo_recv.at[dx - 1], device(z, y, x + dx, c)))
+    p1_start(MIX_OUT)
     p1_start(GATE)
+    p1_ring(UP, 0)
+    p1_ring(DOWN, 0)
 
     def spread_gain(g_ref):
         for r in range(16):
@@ -137,14 +159,6 @@
     )
     r1 = factor(acc1)
 
-    for dx in (1, 3, 2):
-        xs = (x - dx + 4) % 4
-        got = ob.at[b_own, a_own, :, pl.ds(pl.multiple_of(xs * 128, 128), 128)]
-        remote(got, got, xo_send.at[dx - 1], xo_recv.at[dx - 1], device(z, y, x, c)).wait_recv()
-    p1_start(MIX_OUT)
-    p1_start(UP)
-    p1_start(DOWN)
-
     def row_part(t, row, d, way, half):
         if d == 3:
             return bufs[t].at[row, pl.ds(0, 4)] if way == 1 else bufs[t].at[row, pl.ds(4, 4)]
@@ -157,7 +171,7 @@
         row = (b_own - way * (d + arriving) + 16) % 8
         part = row_part(t, row, d, way, half)
         at = d * 2 + half
-        return remote(part, part, p2_send.at[t, w, at], p2_recv.at[t, w, at], ring_b(way))
+        return remote(part, part, p2_send.at[t], p2_recv.at[t, w, at], ring_b(way))
 
     def parts_of(t, d):
         return range(1 if d == 3 else HALVES[t])
@@ -172,7 +186,7 @@
                     p2(t, 2, way, own_half, 1).wait_recv()
                 else:
                     p2(t, 2, way, 0, 1).wait_recv()
-            go(p2(t, d, way, half, 0))
+            p2(t, d, way, half, 0).start()
         if d == 3 and HALVES[t] == 2:
             for way in (1, -1):
                 other_half = 1 if way == 1 else 0
@@ -184,14 +198,42 @@
 
     pair = device(z, y, x, 1 - c)
 
+    xr, xl, xo = (x + 1) % 4, (x + 3) % 4, (x + 2) % 4
+    right, left = device(z, y, x + 1, c), device(z, y, x - 1, c)
+
     def to_pair_row(k):
         row = (b_own - k + 16) % 8
-        return remote(ob.at[row], opb.at[:, row], d2_send.at[k], d2_recv.at[k], pair)
-
-    p1_wait(MIX_IN)
-    forward(MIX_IN, 0)
-    p1_wait(MIX_OUT)
-    forward(MIX_OUT, 0, 0)
+        return remote(ob.at[row], opb.at[:, row], d2_send, d2_recv, pair)
+
+    def x_copy_of(k, chunk, source, way, halved):
+        row = (b_own - k + 16) % 8
+        part = ob.at[row, :, :, lane(source)]
+        if halved:
+            part = ob.at[row, pl.ds(0 if way == 1 else 4, 4), :, lane(source)]
+        at = (1 - way) // 2 + 2 * halved
+        return remote(part, part, xo_send, xo_recv.at[chunk, at], right if way == 1 else left)
+
+    def x_send(k, chunk):
+        for way in (1, -1):
+            x_copy_of(k, chunk, x, way, 0).start()
+
+    def x_wait(chunk, way, halved):
+        rows = pl.ds(0, len(CHUNKS[chunk]))
+        part = ob.at[rows, pl.ds(0, 4 if halved else 8), :, pl.ds(0, 128)]
+        at = (1 - way) // 2 + 2 * halved
+        remote(part, part, xo_send, xo_recv.at[chunk, at], right).wait_recv()
+
+    def x_forward(chunk):
+        for way, source in ((1, xl), (-1, xr)):
+            x_wait(chunk, way, 0)
+            for k in CHUNKS[chunk]:
+                x_copy_of(k, chunk, source, way, 1).start()
+
+    def x_last(chunk):
+        for way in (1, -1):
+            x_wait(chunk, way, 1)
+        for k in CHUNKS[chunk]:
+            to_pair_row(k).start()
 
     def scale_h(src, fac):
         def body(i, carry):
@@ -202,18 +244,38 @@
 
         lax.fori_loop(0, 64, body, 0)
 
+    def both(t, d):
+        forward(t, d, 0)
+        forward(t, d, 1)
+
     scale_h(xb, r1)
+    p1_wait(MIX_IN)
+    forward(MIX_IN, 0)
+    p1_wait(MIX_OUT)
+    forward(MIX_OUT, 0)
+    x_send(0, 0)
+    p1_wait(GATE)
+    forward(GATE, 0, 0)
     forward(MIX_IN, 1)
-    forward(MIX_OUT, 0, 1)
-    go(to_pair_row(0))
+    forward(MIX_OUT, 1)
+    x_send(1, 0)
+    x_send(7, 0)
+    p1_ring(UP, 1)
+    p1_ring(DOWN, 1)
+    forward(GATE, 0, 1)
     forward(MIX_IN, 2)
-    p1_wait(GATE)
-    forward(GATE, 0)
+    forward(MIX_OUT, 2)
+    x_send(2, 1)
+    x_send(6, 1)
+    p1_ring(UP, 2)
+    p1_ring(DOWN, 2)
+    forward(GATE, 1, 0)
     forward(MIX_IN, 3)
-    forward(MIX_OUT, 1, 0)
-    forward(MIX_OUT, 1, 1)
-    go(to_pair_row(1))
-    go(to_pair_row(7))
+    forward(MIX_OUT, 3)
+    x_forward(0)
+    p1_ring(UP, 3)
+    p1_ring(DOWN, 3)
+    forward(GATE, 1, 1)
     spread_gain(g2_ref)
     last(MIX_IN)
 
@@ -231,44 +293,41 @@
         mean = dot(us, band) / counts
         pc[x, :, s * SEQ : (s + 1) * SEQ] = ((mean - us.astype(F32)) * scale_col).astype(BF16)
 
-    right, left = device(z, y, x + 1, c), device(z, y, x - 1, c)
-    xr, xl, xo = (x + 1) % 4, (x + 3) % 4, (x + 2) % 4
-    p1_wait(UP)
-    forward(UP, 0)
-    go(remote(pc.at[x], pc.at[x], p_send.at[0], p_recv.at[0], right))
-    go(remote(pc.at[x], pc.at[x], p_send.at[1], p_recv.at[1], left))
+    lo, hi = pl.ds(0, 64), pl.ds(64, 64)
+    p_own_r = remote(pc.at[x], pc.at[x], p_send.at[0], p_recv.at[0], right)
+    p_own_l = remote(pc.at[x], pc.at[x], p_send.at[1], p_recv.at[1], left)
+    go(p_own_r)
+    go(p_own_l)
     go(remote(pc.at[x], pp.at[x], p_send.at[2], p_recv.at[2], pair))
-    forward(MIX_OUT, 2, 0)
-    forward(MIX_OUT, 2, 1)
-    go(to_pair_row(2))
-    go(to_pair_row(6))
-    forward(GATE, 1)
-    remote(pc.at[xl], pc.at[xl], p_send.at[0], p_recv.at[0], right).wait_recv()
-    lo, hi = pl.ds(0, 64), pl.ds(64, 64)
+    last(MIX_OUT)
+    for k in CHUNKS[2]:
+        x_send(k, 2)
+    p1_ring_last(UP)
+    both(UP, 0)
+    p1_ring_last(DOWN)
+    both(DOWN, 0)
+    x_forward(1)
+    both(GATE, 2)
+    p_own_r.wait_recv()
     go(remote(pc.at[xl, lo], pc.at[xl, lo], p_send.at[3], p_recv.at[3], right))
     go(remote(pc.at[xl], pp.at[xl], p_send.at[4], p_recv.at[4], pair))
-    remote(pc.at[xr], pc.at[xr], p_send.at[1], p_recv.at[1], left).wait_recv()
+    p_own_l.wait_recv()
     go(remote(pc.at[xr, hi], pc.at[xr, hi], p_send.at[5], p_recv.at[5], left))
     go(remote(pc.at[xr], pp.at[xr], p_send.at[6], p_recv.at[6], pair))
-    forward(MIX_OUT, 3)
-    go(to_pair_row(3))
-    go(to_pair_row(5))
-    forward(UP, 1)
-    p1_wait(DOWN)
+    both(UP, 1)
+    x_last(0)
+    both(DOWN, 1)
+    x_forward(2)
+    both(UP, 2)
     remote(pc.at[xo, lo], pc.at[xo, lo], p_send.at[3], p_recv.at[3], right).wait_recv()
     remote(pc.at[xo, hi], pc.at[xo, hi], p_send.at[5], p_recv.at[5], left).wait_recv()
     go(remote(pc.at[xo], pp.at[xo], p_send.at[7], p_recv.at[7], pair))
-    forward(GATE, 2)
-    last(MIX_OUT)
-    go(to_pair_row(4))
-    forward(UP, 2)
-    forward(DOWN, 0, 0)
-    forward(DOWN, 0, 1)
+    x_last(1)
+    x_last(2)
+    both(DOWN, 2)
     for n, at in ((2, x), (4, xl), (6, xr), (7, xo)):
         remote(pc.at[at], pp.at[at], p_send.at[n], p_recv.at[n], pair).wait_recv()
-    for k in range(8):
-        row = (a_own - k + 16) % 8
-        remote(ob.at[row], opb.at[:, row], d2_send.at[k], d2_recv.at[k], pair).wait_recv()
+    remote(ob, opb, d2_send, d2_recv, pair).wait_recv()
 
     def mix_row(b, acc):
         m = dot(ob[b].reshape(256, 512), pc[...].reshape(512, TOK))
@@ -280,27 +339,40 @@
             acc = add_squares(acc, v.astype(F32))
         return acc
 
-    acc2 = lax.fori_loop(0, 8, mix_row, jnp.zeros((8, TOK), F32))
+    acc2 = lax.fori_loop(0, 4, mix_row, jnp.zeros((8, TOK), F32))
     forward(GATE, 3)
+    acc2 = lax.fori_loop(4, 8, mix_row, acc2)
     forward(UP, 3)
-    forward(DOWN, 1, 0)
-    forward(DOWN, 1, 1)
     scale_h(x1b, factor(acc2))
-    forward(DOWN, 2, 0)
-    forward(DOWN, 2, 1)
+
+    def products(steps, first, final):
+        places = [(b_own + k + 8) % 8 for k in steps]
+
+        def half(n, carry):
+            at = pl.ds(pl.multiple_of(n * 256, 256), 256)
+            sums = []
+            for buf, acc in ((gb, g_acc), (ub, u_acc)):
+                total = None if first else acc[:, at]
+                for r in places:
+                    part = dot_first(buf[r].reshape(256, HID), hb[pl.ds(r * 8, 8), :, at].reshape(256, 256))
+                    total = part if total is None else total + part
+                if not final:
+                    acc[:, at] = total
+                sums.append(total)
+            if final:
+                g, v = sums
+                hid[:, at] = (g / (1.0 + jnp.exp(-g)) * v).astype(BF16)
+            return carry
+
+        lax.fori_loop(0, 2, half, 0)
+
+    products((0, 1, -1), True, False)
+    forward(DOWN, 3)
+    products((2, -2), False, False)
+    products((3, -3), False, False)
     last(GATE)
     last(UP)
-    forward(DOWN, 3)
-
-    def hidden_half(n, carry):
-        at = pl.ds(pl.multiple_of(n * 256, 256), 256)
-        rhs = hb[:, :, at].reshape(D, 256)
-        g = dot_first(gb[...].reshape(D, HID), rhs)
-        v = dot_first(ub[...].reshape(D, HID), rhs)
-        hid[:, at] = (g / (1.0 + jnp.exp(-g)) * v).astype(BF16)
-        return carry
-
-    lax.fori_loop(0, 2, hidden_half, 0)
+    products((4,), False, True)
     last(DOWN)
 
     def term(xd, cd):
@@ -344,6 +416,15 @@
     for a in range(8):
         at = slice(a * 32, (a + 1) * 32)
         own[at] = own[at] + from_pair[3, at].astype(F32) + x1b[tp * 8 + a].astype(F32)
+    for t in range(5):
+        seven = bufs[t].at[0, pl.ds(0, 7)]
+        remote(seven, seven, p1_send.at[t], p1_send.at[t], pair).wait_send()
+        rows = bufs[t].at[pl.ds(0, 7)]
+        remote(rows, rows, p2_send.at[t], p2_send.at[t], pair).wait_send()
+    sent = ob.at[pl.ds(0, 6)]
+    remote(sent, sent, xo_send, xo_send, pair).wait_send()
+    remote(ob, opb, d2_send, d2_recv, pair).wait_send()
+    drain(4)
     far_r.wait_recv()
     rgt[0] = (keep_r[...] + in_far[0].astype(F32)).astype(BF16)
     r_sum = remote(rgt.at[0], in_l.at[0], rs_send.at[8], rs_recv.at[8], right)
@@ -364,31 +445,27 @@
     total = jnp.sum(own[...] * own[...], axis=0, keepdims=True)
     ssq[tp] = total
 
-    def q_copy(o, at):
-        t = (tp + o) % 8
-        return remote(ssq.at[at], ssq.at[at], q_send.at[o - 1], q_recv.at[o - 1], device(z, y, t // 2, t % 2))
-
     gain3 = jnp.concatenate(
         [wide(spread_row(g3_ref[pl.ds(tp * 2 + i, 1), :]), 4) for i in range(2)], axis=0
     )
     for o in range(1, 8):
-        go(q_copy(o, tp))
-    for o in range(1, 8):
-        q_copy(o, (tp - o + 8) % 8).wait_recv()
+        t = (tp + o) % 8
+        remote(ssq.at[tp], ssq.at[tp], q_send, q_recv, device(z, y, t // 2, t % 2)).start()
+    seven = ssq.at[pl.ds(0, 7)]
+    squares_copy = remote(seven, seven, q_send, q_recv, pair)
+    squares_copy.wait_recv()
     squares = ssq[0]
     for k in range(1, 8):
         squares = squares + ssq[k]
     fac = lax.rsqrt(squares / D + EPS)
     out_ref[...] = (own[...] * fac * gain3).astype(BF16)
-    for copy in started:
-        copy.wait_send()
+    squares_copy.wait_send()
+    drain(0)
 
 
 def on_device(
     activations, w_mix_in, w_mix_out, w_gate, w_up, w_down, pool_scale, gain_mix, gain_ffn, gain_out
 ):
-    pad = ((0, 0), (0, HID - w_gate.shape[1]))
-    wf = jnp.stack([jnp.pad(w, pad) for w in (w_gate, w_up, w_down)])
     vmem = pl.BlockSpec(memory_space=pltpu.VMEM)
     hbm = pl.BlockSpec(memory_space=pl.ANY)
     dma = pltpu.SemaphoreType.DMA
@@ -396,7 +473,7 @@
     return pl.pallas_call(
         kernel,
         out_shape=jax.ShapeDtypeStruct((256, TOK), BF16),
-        in_specs=[hbm] * 4 + [vmem] * 4,
+        in_specs=[hbm] * 3 + [vmem] * 7,
         out_specs=vmem,
         scratch_shapes=[
             pltpu.VMEM((64, 32, TOK), BF16),
@@ -407,6 +484,8 @@
             pltpu.VMEM((4, 128, TOK), BF16),
             pltpu.VMEM((64, 32, 128), F32),
             pltpu.VMEM((HID, TOK), BF16),
+            pltpu.VMEM((HID, TOK), F32),
+            pltpu.VMEM((HID, TOK), F32),
             pltpu.VMEM((4, 256, TOK), BF16),
             pltpu.VMEM((4, 256, TOK), BF16),
             pltpu.VMEM((256, TOK), F32),
@@ -419,21 +498,21 @@
             pltpu.VMEM((2, 128, TOK), BF16),
             pltpu.VMEM((2, 128, TOK), BF16),
             pltpu.VMEM((8, 1, TOK), F32),
-            dma((6,)),
-            dma((5, 7)), dma((5, 7)),
-            dma((5, 2, 8)), dma((5, 2, 8)),
-            dma((3,)), dma((3,)),
-            dma((8,)), dma((8,)),
+            dma((3,)),
+            dma((5,)), dma((3,)), dma((2, 8)),
+            dma((5,)), dma((5, 2, 8)),
+            dma, dma((3, 4)),
+            dma, dma,
             dma((8,)), dma((8,)),
             dma((10,)), dma((10,)),
-            dma((7,)), dma((7,)),
+            dma, dma,
         ],
         compiler_params=pltpu.CompilerParams(
             collective_id=0, has_side_effects=True, vmem_limit_bytes=60 * 1024 * 1024
         ),
         name="layer",
     )(
-        activations.reshape(64, 32, TOK), w_mix_in, w_mix_out, wf,
+        activations.reshape(64, 32, TOK), w_mix_in, w_mix_out, w_gate, w_up, w_down,
         pool_scale.reshape(8, 128), gain_mix.reshape(16, 128),
         gain_ffn.reshape(16, 128), gain_out.reshape(16, 128),
     )

time: 102 us -> 89 us (0.87)
  Pallas kernels: 98.1 us -> 87.1 us
  local copies, waits for them, and re-layouts: 3.18 us -> 1.67 us
    pallas_call x1, Pallas kernels: 98.1 us -> 87.1 us  [on_device(): pl.pallas_call(kernel, out_shape=jax.ShapeDtypeStruct((256, TOK), BF16),...]
    another operation x2 -> x0, local copies, waits for them, and re-layouts: 1.51 us -> none  [on_device(): wf = jnp.stack([jnp.pad(w, pad) for w in (w_gate, w_up, w_down)])]
where the time goes in v2:
time: 89 us; the launch traced here: 88.7 us
  Pallas kernels  87.1 us (98%)
  local copies, waits for them, and re-layouts  1.67 us (2%)
    pallas_call x1, Pallas kernels, on_device(): pl.pallas_call(kernel, out_shape=jax.ShapeDtypeStruct((256, TOK), BF16),...  87.1 us

profile of v2, /device:TPU:1, one launch (start us, length us, event | category | flops | bytes accessed | tf_op | source)
XLA Modules:
  0.0 88.7 jit_solution(13269411126563133635)
XLA Ops:
  0.0 87.1 %layer.1 = bf16[256,512]{1,0:T(8,128)(2,1)} custom-call(bf16[64,32,512]{2,1,0:T(8,128)(2,1)} %bitcast.5, bf16[32,128]{1,0:T(8,128)(2,1)} %wi_hbm.1, bf16[32,128]{1,0:T(8,128)(2,1)} %wo_hbm.1, bf16[32,352]{1,0:T(8,128)(2,1)} %wg_ref.1, bf16[32,352]{1,0:T(8,128)(2,1)} %wu_ref.1, bf16[32,352]{1,0:T(8,128)(2,1)} %wd_ref.1, f32[8,128]{1,0:T(8,128)} %bitcast.9, ...), custom_call_target="tpu_custom_call" | custom-call | tf_op jit(solution)/shard_map/layer/pallas_call | solution.py:473
  87.1 1.7 %copy.12 = bf16[256,512]{1,0:T(8,128)(2,1)} copy(bf16[256,512]{1,0:T(8,128)(2,1)} %layer.1) | data formatting | bytes 524288

commit v3 on v2

--- a/solution.py
+++ b/solution.py
@@ -35,11 +35,11 @@
 
 
 def kernel(
-    x_hbm, wi_hbm, wo_hbm, wg_ref, wu_ref, wd_ref, scale_ref, g1_ref, g2_ref, g3_ref,
+    x_hbm, wi_hbm, wo_hbm, wg_hbm, wu_hbm, wd_hbm, scale_hbm, g1_hbm, g2_hbm, g3_hbm,
     out_ref,
-    xb, hb, x1b, mb, ob, opb, gb, ub, db, pc, pp, gcol, hid, g_acc, u_acc,
+    xb, hb, x1b, mb, ob, opb, gb, ub, db, pc, pp, gcol, hid, g_acc, u_acc, mix1, w_in, scale_ref, g1_ref, g2_ref, g3_ref,
     to_pair, from_pair, own, far2, rgt, lft, keep_r, keep_l, in_l, in_r, in_far, ssq,
-    loc_sem, p1_send, p1_recv, p1r_recv, p2_send, p2_recv, xo_send, xo_recv, d2_send, d2_recv,
+    loc_sem, p1_send, p1_recv, p1r_recv, p2_send, mo_recv, p2_recv, xo_send, xo_recv, d2_send, d2_recv,
     p_send, p_recv, rs_send, rs_recv, q_send, q_recv,
 ):
     rep, fs, tp = lax.axis_index("rep"), lax.axis_index("fs"), lax.axis_index("tp")
@@ -90,18 +90,30 @@
         ),
     ]
     x_copy = pltpu.make_async_copy(x_hbm, xb, loc_sem.at[2])
-    for cp in locals_:
+    w_copies = [
+        pltpu.make_async_copy(src, w_in.at[i], loc_sem.at[3 + i])
+        for i, src in enumerate((wg_hbm, wu_hbm, wd_hbm))
+    ]
+    small = [
+        pltpu.make_async_copy(src, dst, loc_sem.at[6 + i])
+        for i, (src, dst) in enumerate(
+            ((g1_hbm, g1_ref), (g2_hbm, g2_ref), (g3_hbm, g3_ref), (scale_hbm, scale_ref))
+        )
+    ]
+    for cp in locals_ + w_copies + small:
         cp.start()
     x_copy.start()
     barrier = pltpu.get_barrier_semaphore()
-    peers = [ring_a(d) for d in (1, -1, 2, -2, 3, -3, 4, -4)] + [ring_b(1), ring_b(-1)]
+    peers = [ring_a(d) for d in (1, -1, 2, -2, 3, -3, 4, -4)] + [ring_b(1), ring_b(-1), ring_b(2), ring_b(-2)]
     peers += [device(z, y, x + dx, cc) for dx in (1, 2, 3) for cc in (c, 1 - c)]
     peers += [device(z, y, x, 1 - c)]
     for dev in peers:
         pl.semaphore_signal(barrier, inc=1, device_id=dev, device_id_type=MESH)
-    for buf, ref in ((gb, wg_ref), (ub, wu_ref), (db, wd_ref)):
-        width = ref.shape[1]
-        buf[b_own, a_own, :, 0:width] = ref[...]
+    for cp in w_copies:
+        cp.wait()
+    width = w_in.shape[2]
+    for i, buf in enumerate((gb, ub, db)):
+        buf[b_own, a_own, :, 0:width] = w_in[i]
         buf[b_own, a_own, :, width:HID] = jnp.zeros((32, HID - width), BF16)
     for cp in locals_:
         cp.wait()
@@ -118,29 +130,33 @@
         blks = bufs[t].at[b_own, pl.ds(0, 7)]
         remote(blks, blks, p1_send.at[t], p1_recv.at[t], ring_a(1)).wait_recv()
 
-    def ring_1(t, d, way, arriving):
-        w = (1 - way) // 2
-        at = (a_own - way * (d + arriving) + 16) % 8
+    def ring_1(t, d, way):
+        at = (a_own - way * d + 16) % 8
         blk = bufs[t].at[b_own, at]
         if d == 3:
             blk = bufs[t].at[b_own, at, pl.ds(0 if way == 1 else 16, 16)]
-        return remote(blk, blk, p1_send.at[t], p1r_recv.at[t - UP, w * 4 + d], ring_a(way))
-
-    def p1_ring(t, d):
+        return remote(blk, blk, p1_send.at[t], p1r_recv.at[(1 - way) * 2 + d], ring_a(way))
+
+    def ring_1_wait(d, way):
+        both_types = ub.at[b_own, pl.ds(0, 2)] if d < 3 else ub.at[b_own, 0]
+        sem = p1r_recv.at[(1 - way) * 2 + d]
+        remote(both_types, both_types, p1_send.at[UP], sem, ring_a(way)).wait_recv()
+
+    def p1_ring(d):
         for way in (1, -1):
             if d:
-                ring_1(t, d - 1, way, 1).wait_recv()
-            ring_1(t, d, way, 0).start()
-
-    def p1_ring_last(t):
-        for way in (1, -1):
-            ring_1(t, 3, way, 1).wait_recv()
+                ring_1_wait(d - 1, way)
+            for t in (UP, DOWN):
+                ring_1(t, d, way).start()
+
+    def p1_ring_last():
+        for way in (1, -1):
+            ring_1_wait(3, way)
 
     p1_start(MIX_IN)
     p1_start(MIX_OUT)
     p1_start(GATE)
-    p1_ring(UP, 0)
-    p1_ring(DOWN, 0)
+    p1_ring(0)
 
     def spread_gain(g_ref):
         for r in range(16):
@@ -153,6 +169,8 @@
         return lax.rsqrt(jnp.sum(acc, axis=0, keepdims=True) / D + EPS)
 
     x_copy.wait()
+    for cp in small:
+        cp.wait()
     spread_gain(g1_ref)
     acc1 = lax.fori_loop(
         0, 64, lambda i, acc: add_squares(acc, xb[i].astype(F32)), jnp.zeros((8, TOK), F32)
@@ -171,7 +189,7 @@
         row = (b_own - way * (d + arriving) + 16) % 8
         part = row_part(t, row, d, way, half)
         at = d * 2 + half
-        return remote(part, part, p2_send.at[t], p2_recv.at[t, w, at], ring_b(way))
+        return remote(part, part, p2_send.at[t], p2_recv.at[t - GATE, w, at], ring_b(way))
 
     def parts_of(t, d):
         return range(1 if d == 3 else HALVES[t])
@@ -196,14 +214,40 @@
         for way in (1, -1):
             p2(t, 3, way, 0, 1).wait_recv()
 
+    def jump(t, step, way, arriving):
+        w = (1 - way) // 2
+        hops = (1, 2, 1, 2)[step]
+        held = (0, 0, 2, 2)[step]
+        row = (b_own - way * (held + hops * arriving) + 16) % 8
+        part = bufs[t].at[row]
+        if step == 3:
+            part = bufs[t].at[row, pl.ds(0 if way == 1 else 4, 4)]
+        return remote(part, part, p2_send.at[t], mo_recv.at[t, w, step], ring_b(way * hops))
+
+    def jump_start(t):
+        for step in (1, 0):
+            for way in (1, -1):
+                jump(t, step, way, 0).start()
+
+    def jump_wait(t, step):
+        for way in (1, -1):
+            jump(t, step, way, 1).wait_recv()
+
+    def jump_on(t):
+        for way in (1, -1):
+            jump(t, 1, way, 1).wait_recv()
+            jump(t, 3, way, 0).start()
+            jump(t, 2, way, 0).start()
+
     pair = device(z, y, x, 1 - c)
 
     xr, xl, xo = (x + 1) % 4, (x + 3) % 4, (x + 2) % 4
     right, left = device(z, y, x + 1, c), device(z, y, x - 1, c)
 
-    def to_pair_row(k):
+    def pair_part(k, source):
         row = (b_own - k + 16) % 8
-        return remote(ob.at[row], opb.at[:, row], d2_send, d2_recv, pair)
+        src, dst = ob.at[row, :, :, lane(source)], opb.at[:, row, :, lane(source)]
+        remote(src, dst, d2_send, d2_recv, pair).start()
 
     def x_copy_of(k, chunk, source, way, halved):
         row = (b_own - k + 16) % 8
@@ -216,6 +260,7 @@
     def x_send(k, chunk):
         for way in (1, -1):
             x_copy_of(k, chunk, x, way, 0).start()
+        pair_part(k, x)
 
     def x_wait(chunk, way, halved):
         rows = pl.ds(0, len(CHUNKS[chunk]))
@@ -228,12 +273,14 @@
             x_wait(chunk, way, 0)
             for k in CHUNKS[chunk]:
                 x_copy_of(k, chunk, source, way, 1).start()
+            for k in CHUNKS[chunk]:
+                pair_part(k, source)
 
     def x_last(chunk):
         for way in (1, -1):
             x_wait(chunk, way, 1)
         for k in CHUNKS[chunk]:
-            to_pair_row(k).start()
+            pair_part(k, xo)
 
     def scale_h(src, fac):
         def body(i, carry):
@@ -250,34 +297,27 @@
 
     scale_h(xb, r1)
     p1_wait(MIX_IN)
-    forward(MIX_IN, 0)
+    jump_start(MIX_IN)
     p1_wait(MIX_OUT)
-    forward(MIX_OUT, 0)
+    jump_start(MIX_OUT)
     x_send(0, 0)
     p1_wait(GATE)
     forward(GATE, 0, 0)
-    forward(MIX_IN, 1)
-    forward(MIX_OUT, 1)
+    p1_ring(1)
+    jump_on(MIX_IN)
+    jump_on(MIX_OUT)
+    x_send(2, 1)
+    x_send(6, 1)
+    jump_wait(MIX_OUT, 0)
     x_send(1, 0)
     x_send(7, 0)
-    p1_ring(UP, 1)
-    p1_ring(DOWN, 1)
     forward(GATE, 0, 1)
-    forward(MIX_IN, 2)
-    forward(MIX_OUT, 2)
-    x_send(2, 1)
-    x_send(6, 1)
-    p1_ring(UP, 2)
-    p1_ring(DOWN, 2)
+    p1_ring(2)
     forward(GATE, 1, 0)
-    forward(MIX_IN, 3)
-    forward(MIX_OUT, 3)
-    x_forward(0)
-    p1_ring(UP, 3)
-    p1_ring(DOWN, 3)
-    forward(GATE, 1, 1)
     spread_gain(g2_ref)
-    last(MIX_IN)
+    jump_wait(MIX_IN, 0)
+    jump_wait(MIX_IN, 2)
+    jump_wait(MIX_IN, 3)
 
     u = dot_first(mb[...].reshape(D, 128), hb[...].reshape(D, TOK)).astype(BF16)
     behind = lax.shift_left(jnp.int32(1), x.astype(jnp.int32))
@@ -299,12 +339,15 @@
     go(p_own_r)
     go(p_own_l)
     go(remote(pc.at[x], pp.at[x], p_send.at[2], p_recv.at[2], pair))
-    last(MIX_OUT)
+    jump_wait(MIX_OUT, 2)
+    jump_wait(MIX_OUT, 3)
     for k in CHUNKS[2]:
         x_send(k, 2)
-    p1_ring_last(UP)
+    p1_ring(3)
+    forward(GATE, 1, 1)
+    x_forward(0)
+    p1_ring_last()
     both(UP, 0)
-    p1_ring_last(DOWN)
     both(DOWN, 0)
     x_forward(1)
     both(GATE, 2)
@@ -318,20 +361,27 @@
     x_last(0)
     both(DOWN, 1)
     x_forward(2)
+    x_last(1)
     both(UP, 2)
     remote(pc.at[xo, lo], pc.at[xo, lo], p_send.at[3], p_recv.at[3], right).wait_recv()
     remote(pc.at[xo, hi], pc.at[xo, hi], p_send.at[5], p_recv.at[5], left).wait_recv()
     go(remote(pc.at[xo], pp.at[xo], p_send.at[7], p_recv.at[7], pair))
-    x_last(1)
+
+    def mix_own(i, carry):
+        row = (b_own + 6 + i) % 8
+        mix1[row] = dot(ob[row].reshape(256, 512), pc[...].reshape(512, TOK))
+        return carry
+
+    lax.fori_loop(0, 5, mix_own, 0)
     x_last(2)
     both(DOWN, 2)
+    lax.fori_loop(5, 8, mix_own, 0)
     for n, at in ((2, x), (4, xl), (6, xr), (7, xo)):
         remote(pc.at[at], pp.at[at], p_send.at[n], p_recv.at[n], pair).wait_recv()
     remote(ob, opb, d2_send, d2_recv, pair).wait_recv()
 
     def mix_row(b, acc):
-        m = dot(ob[b].reshape(256, 512), pc[...].reshape(512, TOK))
-        m = m + dot(opb[b].reshape(256, 512), pp[...].reshape(512, TOK))
+        m = mix1[b] + dot(opb[b].reshape(256, 512), pp[...].reshape(512, TOK))
         for a in range(8):
             f = fidx(b, a)
             v = (xb[f].astype(F32) + m[a * 32 : (a + 1) * 32]).astype(BF16)
@@ -339,10 +389,11 @@
             acc = add_squares(acc, v.astype(F32))
         return acc
 
+    forward(GATE, 3)
+    forward(UP, 3)
     acc2 = lax.fori_loop(0, 4, mix_row, jnp.zeros((8, TOK), F32))
-    forward(GATE, 3)
+    forward(DOWN, 3)
     acc2 = lax.fori_loop(4, 8, mix_row, acc2)
-    forward(UP, 3)
     scale_h(x1b, factor(acc2))
 
     def products(steps, first, final):
@@ -366,10 +417,7 @@
 
         lax.fori_loop(0, 2, half, 0)
 
-    products((0, 1, -1), True, False)
-    forward(DOWN, 3)
-    products((2, -2), False, False)
-    products((3, -3), False, False)
+    products((0, 1, -1, 2, -2, 3, -3), True, False)
     last(GATE)
     last(UP)
     products((4,), False, True)
@@ -473,7 +521,7 @@
     return pl.pallas_call(
         kernel,
         out_shape=jax.ShapeDtypeStruct((256, TOK), BF16),
-        in_specs=[hbm] * 3 + [vmem] * 7,
+        in_specs=[hbm] * 10,
         out_specs=vmem,
         scratch_shapes=[
             pltpu.VMEM((64, 32, TOK), BF16),
@@ -486,6 +534,12 @@
             pltpu.VMEM((HID, TOK), BF16),
             pltpu.VMEM((HID, TOK), F32),
             pltpu.VMEM((HID, TOK), F32),
+            pltpu.VMEM((8, 256, TOK), F32),
+            pltpu.VMEM((3, *w_gate.shape), BF16),
+            pltpu.VMEM((8, 128), F32),
+            pltpu.VMEM((16, 128), F32),
+            pltpu.VMEM((16, 128), F32),
+            pltpu.VMEM((16, 128), F32),
             pltpu.VMEM((4, 256, TOK), BF16),
             pltpu.VMEM((4, 256, TOK), BF16),
             pltpu.VMEM((256, TOK), F32),
@@ -498,9 +552,9 @@
             pltpu.VMEM((2, 128, TOK), BF16),
             pltpu.VMEM((2, 128, TOK), BF16),
             pltpu.VMEM((8, 1, TOK), F32),
-            dma((3,)),
-            dma((5,)), dma((3,)), dma((2, 8)),
-            dma((5,)), dma((5, 2, 8)),
+            dma((10,)),
+            dma((5,)), dma((3,)), dma((8,)),
+            dma((5,)), dma((2, 2, 4)), dma((3, 2, 7)),
             dma, dma((3, 4)),
             dma, dma,
             dma((8,)), dma((8,)),

time: 89 us -> 86.9 us (0.976)
  Pallas kernels: 87.1 us -> 85 us
    pallas_call x1, Pallas kernels: 87.1 us -> 85 us  [on_device(): pl.pallas_call(kernel, out_shape=jax.ShapeDtypeStruct((256, TOK), BF16),...]
where the time goes in v3:
time: 86.9 us; the launch traced here: 86.7 us
  Pallas kernels  85 us (98%)
  local copies, waits for them, and re-layouts  1.67 us (2%)
    pallas_call x1, Pallas kernels, on_device(): pl.pallas_call(kernel, out_shape=jax.ShapeDtypeStruct((256, TOK), BF16),...  85 us

profile of v3, /device:TPU:1, one launch (start us, length us, event | category | flops | bytes accessed | tf_op | source)
XLA Modules:
  0.0 86.7 jit_solution(9836836196657957010)
XLA Ops:
  0.0 85.0 %layer.1 = bf16[256,512]{1,0:T(8,128)(2,1)} custom-call(bf16[64,32,512]{2,1,0:T(8,128)(2,1)} %bitcast.5, bf16[32,128]{1,0:T(8,128)(2,1)} %wi_hbm.1, bf16[32,128]{1,0:T(8,128)(2,1)} %wo_hbm.1, bf16[32,352]{1,0:T(8,128)(2,1)} %wg_hbm.1, bf16[32,352]{1,0:T(8,128)(2,1)} %wu_hbm.1, bf16[32,352]{1,0:T(8,128)(2,1)} %wd_hbm.1, f32[8,128]{1,0:T(8,128)} %bitcast.9, ...), custom_call_target="tpu_custom_call" | custom-call | tf_op jit(solution)/shard_map/layer/pallas_call | solution.py:521
  85.0 1.7 %copy.12 = bf16[256,512]{1,0:T(8,128)(2,1)} copy(bf16[256,512]{1,0:T(8,128)(2,1)} %layer.1) | data formatting | bytes 524288
